TPU v7x, 1024 devices: a whole 4x4x32 slice. The times are simulated.
1024 devices in a mesh: sp: 64 (over z, core), tp: 16 (over y, x).
Axes of the slice: x: 4, y: 4, z: 32, core: 2. Of those that a mesh axis runs over, the one named last changes fastest.
Arguments:
- decoder_inputs: bfloat16 [8192, 2048], P('sp', 'tp'), may hold values from -300 to 300
- encoder_states: bfloat16 [16384, 2048], P('sp'), may hold values from -6 to 6
- rescale_coefficients: float32 [3, 2048], replicated, may hold values from 0.1 to 1.9
- encoder_rescale: float32 [2, 2048], replicated, may hold values from 0.1 to 1.9
- asking_weights: bfloat16 [2, 2048, 2048], P(None, None, 'tp'), may hold values from -0.125 to 0.125
- lookup_weights: bfloat16 [2, 2048, 256], P(None, None, 'tp'), may hold values from -0.125 to 0.125
- content_weights: bfloat16 [2, 2048, 256], P(None, None, 'tp'), may hold values from -0.125 to 0.125
- merging_weights: bfloat16 [2, 2048, 2048], P(None, None, 'tp'), may hold values from -0.25 to 0.25
- sharpness_factors: float32 [2, 16], replicated, may hold values from 1 to 60
- switching_weights: bfloat16 [2048, 6144], P(None, 'tp'), may hold values from -0.125 to 0.125
- expanding_weights: bfloat16 [2048, 6144], P(None, 'tp'), may hold values from -0.125 to 0.125
- contracting_weights: bfloat16 [6144, 2048], P(None, 'tp'), may hold values from -0.078125 to 0.078125
Outputs:
- updated: bfloat16 [8192, 2048], P('sp', 'tp')
All inputs are finite; a program needn't handle non-finite values.
Results may differ from a plain program's by a relative error of at most 0.024.
Values may be sent and summed in bfloat16 or wider, within the bound.
A program may use at most 64 MiB of HBM per device.

v0:
```python
import math

import jax
import jax.numpy as jnp
from jax import lax
from jax.sharding import PartitionSpec as P

D = 2048
CHANNEL_WIDTH = 128
QH = 16
SHARED_LOOKUPS = 2


EPSILON = 1e-06


def shortened(value):
    return jax.tree.map(lambda a: a.astype(jnp.bfloat16) if a.dtype == jnp.float32 else a, value)


def in_one_piece(arrays, axis, dim, along):
    both = jnp.concatenate(arrays, axis=along)
    result, at, outs = (lax.all_gather(both, axis, axis=dim, tiled=True), 0, [])
    for a in arrays:
        outs.append(lax.slice_in_dim(result, at, at + a.shape[along], axis=along))
        at += a.shape[along]
    return tuple(outs)


def laid_out(parts, dim):
    parts = jnp.moveaxis(parts, 0, dim)
    dims = parts.shape
    return parts.reshape(*dims[:dim], dims[dim] * dims[dim + 1], *dims[dim + 2 :])


def from_everyone(value, axis):
    copies = jnp.broadcast_to(value, (lax.axis_size(axis), *value.shape))
    return lax.all_to_all(copies, axis, split_axis=0, concat_axis=0, tiled=True)


def gathered_copies(value, axis, dim):
    return laid_out(from_everyone(value, axis), dim)


def regroup(items):
    return jax.tree.map(
        lambda part, own: part.astype(own.dtype),
        lax.all_to_all(shortened(items), "tp", split_axis=0, concat_axis=1, tiled=True),
        items,
    )


def fold_sources(pieces, step_fn, initial):
    return step_fn(
        initial,
        in_one_piece((pieces[0], pieces[1], pieces[2], pieces[3]), "sp", 0, 1),
        jnp.int32(0),
    )


def fold_columns(value, gain, weights):
    row_count = value.shape[0]
    initial = (
        tuple((jnp.zeros((row_count, weight.shape[1]), jnp.float32) for weight in weights)),
        jnp.zeros((row_count,), jnp.float32),
    )
    portion = gathered_copies(value, "tp", 1)
    if gain is None:
        operand = portion
        squares = initial[1]
    else:
        widened = portion.astype(jnp.float32)
        operand = (widened * gain).astype(jnp.bfloat16)
        squares = jnp.sum(widened * widened, axis=1)
    products = tuple(
        (jnp.dot(operand, weight, preferred_element_type=jnp.float32) for weight in weights)
    )
    return (products, squares)


def attend(softmax_state, key_piece, value_piece, grouped, softmax_factor):
    weighted, maxima, totals = softmax_state
    key_count = key_piece.shape[0]
    key_heads = key_piece.reshape(key_count, SHARED_LOOKUPS, CHANNEL_WIDTH)
    value_heads = value_piece.reshape(key_count, SHARED_LOOKUPS, CHANNEL_WIDTH)
    scores = jnp.einsum("tgrd,kgd->grkt", grouped, key_heads, preferred_element_type=jnp.float32)
    scores = scores * softmax_factor[:, :, None, None]
    new_maxima = jnp.maximum(maxima, jnp.max(scores, axis=2))
    shrink = jnp.exp(maxima - new_maxima)
    expwts = jnp.exp(scores - new_maxima[:, :, None, :])
    totals = totals * shrink + jnp.sum(expwts, axis=2)
    weighted = weighted * shrink[:, :, None, :] + jnp.einsum(
        "grkt,kgd->grdt",
        expwts.astype(jnp.bfloat16),
        value_heads,
        preferred_element_type=jnp.float32,
    )
    return (weighted, new_maxima, totals)


def attend_blocks(softmax_state, key_buffer, value_buffer, grouped, softmax_factor):
    total_rows = key_buffer.shape[0]
    block_rows = math.gcd(total_rows, 256)
    block_count = total_rows // block_rows
    key_blocks = key_buffer.reshape(block_count, block_rows, key_buffer.shape[1])
    value_blocks = value_buffer.reshape(block_count, block_rows, value_buffer.shape[1])

    def attend_step(state, pair):
        return (attend(state, pair[0], pair[1], grouped, softmax_factor), None)

    final_state, unused = lax.scan(attend_step, softmax_state, (key_blocks, value_blocks))
    return final_state


def collect(carried, portion, offset):
    return tuple((piece for piece in portion))


def finish(softmax_state, tp_count, row_count):
    weighted, maxima, totals = softmax_state
    shares = (
        (weighted / totals[:, :, None, :])
        .astype(jnp.bfloat16)
        .reshape(QH * CHANNEL_WIDTH, row_count)
    )
    partials = regroup(shares)
    got_maxima, got_totals = (
        lax.all_to_all(
            maxima.reshape(QH, row_count), "tp", split_axis=0, concat_axis=1, tiled=True
        ),
        lax.all_to_all(
            totals.reshape(QH, row_count), "tp", split_axis=0, concat_axis=1, tiled=True
        ),
    )
    own_heads = QH // tp_count
    got_maxima = got_maxima.reshape(own_heads, tp_count, row_count)
    largest = jnp.max(got_maxima, axis=1, keepdims=True)
    mixing = jnp.exp(got_maxima - largest) * got_totals.reshape(own_heads, tp_count, row_count)
    mixing = mixing / jnp.sum(mixing, axis=1, keepdims=True)
    merged = jnp.einsum(
        "hdjt,hjt->thd",
        partials.reshape(own_heads, CHANNEL_WIDTH, tp_count, row_count).astype(jnp.float32),
        mixing,
    )
    return merged.reshape(row_count, own_heads * CHANNEL_WIDTH).astype(jnp.bfloat16)


def per_device(
    decoder_inputs,
    encoder_states,
    rescale_coefficients,
    encoder_rescale,
    asking_weights,
    lookup_weights,
    content_weights,
    merging_weights,
    sharpness_factors,
    switching_weights,
    expanding_weights,
    contracting_weights,
):
    tp_count = lax.axis_size("tp")
    row_count = decoder_inputs.shape[0]
    askers_sharing_lookup = QH // SHARED_LOOKUPS
    widened = encoder_states.astype(jnp.float32)
    source_scale = lax.rsqrt(jnp.mean(widened * widened, axis=1, keepdims=True) + EPSILON)
    projected = []
    for tier_index in range(2):
        normed = (widened * encoder_rescale[tier_index]).astype(jnp.bfloat16)
        for weight in (lookup_weights[tier_index], content_weights[tier_index]):
            product = jnp.dot(normed, weight, preferred_element_type=jnp.float32)
            projected.append((product * source_scale).astype(jnp.bfloat16))
    kv_rows = regroup(tuple(projected))
    holder = jnp.zeros(
        (lax.axis_size("sp") * kv_rows[0].shape[0], kv_rows[0].shape[1]), jnp.bfloat16
    )
    stream = decoder_inputs
    kept_keys = None
    kept_values = None
    for tier_index in range(2):
        products, squares = fold_columns(
            stream, rescale_coefficients[tier_index], (asking_weights[tier_index],)
        )
        scaling = lax.rsqrt(squares / D + EPSILON)[:, None]
        own_queries = (products[0] * scaling).astype(jnp.bfloat16)
        all_queries = gathered_copies(own_queries, "tp", 1)
        grouped = all_queries.reshape(
            row_count, SHARED_LOOKUPS, askers_sharing_lookup, CHANNEL_WIDTH
        )
        softmax_factor = (sharpness_factors[tier_index] * CHANNEL_WIDTH ** (-0.5)).reshape(
            SHARED_LOOKUPS, askers_sharing_lookup
        )
        initial = (
            jnp.zeros(
                (SHARED_LOOKUPS, askers_sharing_lookup, CHANNEL_WIDTH, row_count), jnp.float32
            ),
            jnp.full((SHARED_LOOKUPS, askers_sharing_lookup, row_count), -1e30, jnp.float32),
            jnp.zeros((SHARED_LOOKUPS, askers_sharing_lookup, row_count), jnp.float32),
        )
        encoder_lookups = kv_rows[2 * tier_index]
        encoder_contents = kv_rows[2 * tier_index + 1]
        if tier_index == 0:
            key_buffer, value_buffer, kept_keys, kept_values = fold_sources(
                (encoder_lookups, encoder_contents, kv_rows[2], kv_rows[3]),
                collect,
                (holder, holder, holder, holder),
            )
        else:
            key_buffer, value_buffer = (kept_keys, kept_values)
        softmax_state = attend_blocks(initial, key_buffer, value_buffer, grouped, softmax_factor)
        mixed_entries = finish(softmax_state, tp_count, row_count)
        products, squares = fold_columns(mixed_entries, None, (merging_weights[tier_index],))
        stream = (stream.astype(jnp.float32) + products[0]).astype(jnp.bfloat16)
    products, squares = fold_columns(
        stream, rescale_coefficients[2], (switching_weights, expanding_weights)
    )
    scaling = lax.rsqrt(squares / D + EPSILON)[:, None]
    hidden = (jax.nn.silu(products[0] * scaling) * (products[1] * scaling)).astype(jnp.bfloat16)
    products, squares = fold_columns(hidden, None, (contracting_weights,))
    return (stream.astype(jnp.float32) + products[0]).astype(jnp.bfloat16)


def solution(mesh):
    placed = (
        P("sp", "tp"),
        P("sp", None),
        P(),
        P(),
        P(None, None, "tp"),
        P(None, None, "tp"),
        P(None, None, "tp"),
        P(None, None, "tp"),
        P(),
        P(None, "tp"),
        P(None, "tp"),
        P(None, "tp"),
    )
    return jax.shard_map(
        per_device, mesh=mesh, in_specs=placed, out_specs=P("sp", "tp"), check_vma=False
    )
```

profile of v0, /device:TPU:2, one launch (start us, length us, event | category | flops | bytes accessed | tf_op | source)
XLA Modules:
  0.0 462.9 jit_solution(14905132915170599302)
XLA Ops:
  6.5 1.7 fusion.17
  9.0 1.6 fusion.26
  11.5 16.4 %all-to-all-start = ((bf16[16,2,128]{2,1,0:T(2,128)(2,1)}), bf16[16,2,128]{2,1,0:T(2,128)(2,1)S(1)}, u32[]{:S(2)}, u32[]{:S(2)}) async-start(bf16[16,2,128]{2,1,0:T(2,128)(2,1)} %reshape.363), calls=%async_computation | async-start | bytes 16384 | tf_op jit(solution)/shard_map/all_to_all | solution.py:48
  29.1 4.9 %all-to-all-done = bf16[16,2,128]{2,1,0:T(2,128)(2,1)S(1)} async-done(((bf16[16,2,128]{2,1,0:T(2,128)(2,1)}), bf16[16,2,128]{2,1,0:T(2,128)(2,1)S(1)}, u32[]{:S(2)}, u32[]{:S(2)}) %all-to-all-start) | async-done | bytes 8224 | tf_op jit(solution)/shard_map/all_to_all | solution.py:48
  34.0 4.9 %all-to-all-start.1 = ((bf16[16,2,128]{2,1,0:T(2,128)(2,1)}), bf16[16,2,128]{2,1,0:T(2,128)(2,1)S(1)}, u32[]{:S(2)}, u32[]{:S(2)}) async-start(bf16[16,2,128]{2,1,0:T(2,128)(2,1)} %reshape.361), calls=%async_computation.1 | async-start | bytes 16384 | tf_op jit(solution)/shard_map/all_to_all | solution.py:48
  40.1 5.0 %all-to-all-done.1 = bf16[16,2,128]{2,1,0:T(2,128)(2,1)S(1)} async-done(((bf16[16,2,128]{2,1,0:T(2,128)(2,1)}), bf16[16,2,128]{2,1,0:T(2,128)(2,1)S(1)}, u32[]{:S(2)}, u32[]{:S(2)}) %all-to-all-start.1) | async-done | bytes 8224 | tf_op jit(solution)/shard_map/all_to_all | solution.py:48
  45.1 4.7 %all-to-all-start.2 = ((bf16[16,2,128]{2,1,0:T(2,128)(2,1)}), bf16[16,2,128]{2,1,0:T(2,128)(2,1)S(1)}, u32[]{:S(2)}, u32[]{:S(2)}) async-start(bf16[16,2,128]{2,1,0:T(2,128)(2,1)} %reshape.359), calls=%async_computation.2 | async-start | bytes 16384 | tf_op jit(solution)/shard_map/all_to_all | solution.py:48
  51.0 4.9 %all-to-all-done.2 = bf16[16,2,128]{2,1,0:T(2,128)(2,1)S(1)} async-done(((bf16[16,2,128]{2,1,0:T(2,128)(2,1)}), bf16[16,2,128]{2,1,0:T(2,128)(2,1)S(1)}, u32[]{:S(2)}, u32[]{:S(2)}) %all-to-all-start.2) | async-done | bytes 8224 | tf_op jit(solution)/shard_map/all_to_all | solution.py:48
  55.9 4.9 %all-to-all-start.3 = ((bf16[16,2,128]{2,1,0:T(2,128)(2,1)}), bf16[16,2,128]{2,1,0:T(2,128)(2,1)S(1)}, u32[]{:S(2)}, u32[]{:S(2)}) async-start(bf16[16,2,128]{2,1,0:T(2,128)(2,1)} %reshape.357), calls=%async_computation.3 | async-start | bytes 16384 | tf_op jit(solution)/shard_map/all_to_all | solution.py:48
  61.6 5.4 %all-to-all-done.3 = bf16[16,2,128]{2,1,0:T(2,128)(2,1)S(1)} async-done(((bf16[16,2,128]{2,1,0:T(2,128)(2,1)}), bf16[16,2,128]{2,1,0:T(2,128)(2,1)S(1)}, u32[]{:S(2)}, u32[]{:S(2)}) %all-to-all-start.3) | async-done | bytes 8224 | tf_op jit(solution)/shard_map/all_to_all | solution.py:48
  68.9 4.9 %all-to-all-start.4 = ((bf16[16,128,128]{1,2,0:T(8,128)(2,1)}), bf16[16,128,128]{1,2,0:T(8,128)(2,1)S(1)}, u32[]{:S(2)}, u32[]{:S(2)}) async-start(bf16[16,128,128]{1,2,0:T(8,128)(2,1)} %broadcast_in_dim.20), calls=%async_computation.4 | async-start | bytes 1048576 | tf_op jit(solution)/shard_map/all_to_all | solution.py:38
  74.5 11.2 %all-to-all-done.4 = bf16[16,128,128]{1,2,0:T(8,128)(2,1)S(1)} async-done(((bf16[16,128,128]{1,2,0:T(8,128)(2,1)}), bf16[16,128,128]{1,2,0:T(8,128)(2,1)S(1)}, u32[]{:S(2)}, u32[]{:S(2)}) %all-to-all-start.4) | async-done | bytes 524320 | tf_op jit(solution)/shard_map/all_to_all | solution.py:38
  86.0 1.4 fusion.21
  88.3 4.9 %all-to-all-start.5 = ((bf16[16,128,128]{2,1,0:T(8,128)(2,1)}), bf16[16,128,128]{2,1,0:T(8,128)(2,1)S(1)}, u32[]{:S(2)}, u32[]{:S(2)}) async-start(bf16[16,128,128]{2,1,0:T(8,128)(2,1)} %broadcast_in_dim.21), calls=%async_computation.5 | async-start | bytes 1048576 | tf_op jit(solution)/shard_map/all_to_all | solution.py:38
  93.8 106.7 %all-gather.2.cloned.1.call-done = bf16[1024,1024]{1,0:T(8,128)(2,1)} async-done(((bf16[16,1024]{1,0:T(8,128)(2,1)}), bf16[1024,1024]{1,0:T(8,128)(2,1)}) %all-gather.2.cloned.1.call-update) | async-done | bytes 2097168 | tf_op jit(solution)/shard_map/all_gather | solution.py:23
  200.5 2.9 fusion.59
  203.4 36.9 %while.30 = (s32[]{:T(128)}, f32[2,8,128,128]{3,2,1,0:T(8,128)S(1)}, f32[2,8,128]{2,1,0:T(8,128)S(1)}, f32[2,8,128]{2,1,0:T(8,128)}, bf16[4,256,256]{2,1,0:T(8,1...) while((s32[]{:T(128)}, ...), condition=%wide.region_5.6_spmd.clone, body=%wide.region_2.5_spmd.clone.sunk | while | flops 273426432 | bytes 10355125 | solution.py:111
  205.2 1.8 bitcast_reduce_fusion.4
  207.0 2.0 fusion.96
  209.8 2.3 fusion.98
  213.9 1.8 bitcast_reduce_fusion.4
  215.7 2.0 fusion.96
  219.2 2.3 fusion.98
  223.3 1.8 bitcast_reduce_fusion.4
  225.1 2.0 fusion.96
  228.6 2.3 fusion.98
  232.7 1.8 bitcast_reduce_fusion.4
  234.5 2.0 fusion.96
  238.0 2.3 fusion.98
  240.3 13.3 %all_to_all.206 = f32[16,1,128]{2,1,0:T(1,128)S(1)} all-to-all(f32[16,1,128]{2,1,0:T(1,128)S(1)} %bitcast.225), channel_id=1, replica_groups=mesh['sp'=64,'tp'=16] {'tp'}, dimensions={0} | all-to-all | bytes 16384 | tf_op jit(solution)/shard_map/all_to_all | solution.py:128
  253.6 4.6 %all-to-all-start.8 = ((f32[16,1,128]{2,1,0:T(1,128)}), f32[16,1,128]{2,1,0:T(1,128)S(1)}, u32[]{:S(2)}, u32[]{:S(2)}) async-start(f32[16,1,128]{2,1,0:T(1,128)} %bitcast.30), calls=%async_computation.8 | async-start | bytes 16384 | tf_op jit(solution)/shard_map/all_to_all | solution.py:131
  258.2 1.6 divide_convert_fusion.1
  259.8 4.5 all-to-all-done.8
  264.3 5.0 %all-to-all-start.6 = ((bf16[16,128,128]{2,1,0:T(8,128)(2,1)}), bf16[16,128,128]{2,1,0:T(8,128)(2,1)S(1)}, u32[]{:S(2)}, u32[]{:S(2)}) async-start(bf16[16,128,128]{2,1,0:T(8,128)(2,1)} %bitcast.27), calls=%async_computation.6 | async-start | bytes 1048576 | tf_op jit(solution)/shard_map/all_to_all | solution.py:48
  269.4 8.8 %all-to-all-done.6 = bf16[16,128,128]{2,1,0:T(8,128)(2,1)S(1)} async-done(((bf16[16,128,128]{2,1,0:T(8,128)(2,1)}), bf16[16,128,128]{2,1,0:T(8,128)(2,1)S(1)}, u32[]{:S(2)}, u32[]{:S(2)}) %all-to-all-start.6) | async-done | bytes 524320 | tf_op jit(solution)/shard_map/all_to_all | solution.py:48
  278.4 13.1 %all_to_all.207 = bf16[16,128,128]{1,2,0:T(8,128)(2,1)S(1)} all-to-all(bf16[16,128,128]{1,2,0:T(8,128)(2,1)S(1)} %broadcast_in_dim.22), channel_id=1, replica_groups=mesh['sp'=64,'tp'=16] {'tp'}, dimensions={0} | all-to-all | bytes 1048576 | tf_op jit(solution)/shard_map/all_to_all | solution.py:38
  291.5 1.4 fusion.22
  293.1 13.1 %all_to_all.208 = bf16[16,128,128]{1,2,0:T(8,128)(2,1)S(1)} all-to-all(bf16[16,128,128]{1,2,0:T(8,128)(2,1)S(1)} %broadcast_in_dim.23), channel_id=1, replica_groups=mesh['sp'=64,'tp'=16] {'tp'}, dimensions={0} | all-to-all | bytes 1048576 | tf_op jit(solution)/shard_map/all_to_all | solution.py:38
  306.5 1.4 fusion.23
  308.8 4.8 %all-to-all-start.11 = ((bf16[16,128,128]{2,1,0:T(8,128)(2,1)}), bf16[16,128,128]{2,1,0:T(8,128)(2,1)S(1)}, u32[]{:S(2)}, u32[]{:S(2)}) async-start(bf16[16,128,128]{2,1,0:T(8,128)(2,1)} %broadcast_in_dim.24), calls=%async_computation.11 | async-start | bytes 1048576 | tf_op jit(solution)/shard_map/all_to_all | solution.py:38
  313.7 8.8 %all-to-all-done.11 = bf16[16,128,128]{2,1,0:T(8,128)(2,1)S(1)} async-done(((bf16[16,128,128]{2,1,0:T(8,128)(2,1)}), bf16[16,128,128]{2,1,0:T(8,128)(2,1)S(1)}, u32[]{:S(2)}, u32[]{:S(2)}) %all-to-all-start.11) | async-done | bytes 524320 | tf_op jit(solution)/shard_map/all_to_all | solution.py:38
  322.5 37.1 %while.31 = (s32[]{:T(128)}, f32[2,8,128,128]{3,2,1,0:T(8,128)S(1)}, f32[2,8,128]{2,1,0:T(8,128)S(1)}, f32[2,8,128]{2,1,0:T(8,128)}, bf16[4,256,256]{2,1,0:T(8,1...) while((s32[]{:T(128)}, ...), condition=%wide.region_12.13_spmd.clone, body=%wide.region_9.12_spmd.clone.sunk | while | flops 273426432 | bytes 10355125 | solution.py:111
  324.4 1.8 bitcast_reduce_fusion.5
  326.2 2.0 fusion.103
  328.9 2.3 fusion.105
  333.1 1.8 bitcast_reduce_fusion.5
  335.0 2.0 fusion.103
  338.4 2.3 fusion.105
  342.6 1.8 bitcast_reduce_fusion.5
  344.4 2.0 fusion.103
  347.8 2.3 fusion.105
  352.0 1.8 bitcast_reduce_fusion.5
  353.9 2.0 fusion.103
  357.3 2.3 fusion.105
  359.6 10.5 %all_to_all.209 = f32[16,1,128]{2,1,0:T(1,128)S(1)} all-to-all(f32[16,1,128]{2,1,0:T(1,128)S(1)} %bitcast.226), channel_id=1, replica_groups=mesh['sp'=64,'tp'=16] {'tp'}, dimensions={0} | all-to-all | bytes 16384 | tf_op jit(solution)/shard_map/all_to_all | solution.py:128
  370.2 4.8 %all-to-all-start.14 = ((f32[16,1,128]{2,1,0:T(1,128)}), f32[16,1,128]{2,1,0:T(1,128)S(1)}, u32[]{:S(2)}, u32[]{:S(2)}) async-start(f32[16,1,128]{2,1,0:T(1,128)} %bitcast.49), calls=%async_computation.14 | async-start | bytes 16384 | tf_op jit(solution)/shard_map/all_to_all | solution.py:131
  375.0 1.6 divide_convert_fusion
  376.6 5.1 %all-to-all-done.14 = f32[16,1,128]{2,1,0:T(1,128)S(1)} async-done(((f32[16,1,128]{2,1,0:T(1,128)}), f32[16,1,128]{2,1,0:T(1,128)S(1)}, u32[]{:S(2)}, u32[]{:S(2)}) %all-to-all-start.14) | async-done | bytes 8224 | tf_op jit(solution)/shard_map/all_to_all | solution.py:131
  381.8 5.0 %all-to-all-start.12 = ((bf16[16,128,128]{2,1,0:T(8,128)(2,1)}), bf16[16,128,128]{2,1,0:T(8,128)(2,1)S(1)}, u32[]{:S(2)}, u32[]{:S(2)}) async-start(bf16[16,128,128]{2,1,0:T(8,128)(2,1)} %bitcast.46), calls=%async_computation.12 | async-start | bytes 1048576 | tf_op jit(solution)/shard_map/all_to_all | solution.py:48
  386.9 11.6 %all-to-all-done.12 = bf16[16,128,128]{2,1,0:T(8,128)(2,1)S(1)} async-done(((bf16[16,128,128]{2,1,0:T(8,128)(2,1)}), bf16[16,128,128]{2,1,0:T(8,128)(2,1)S(1)}, u32[]{:S(2)}, u32[]{:S(2)}) %all-to-all-start.12) | async-done | bytes 524320 | tf_op jit(solution)/shard_map/all_to_all | solution.py:48
  398.7 16.2 %all_to_all.210 = bf16[16,128,128]{1,2,0:T(8,128)(2,1)S(1)} all-to-all(bf16[16,128,128]{1,2,0:T(8,128)(2,1)S(1)} %broadcast_in_dim.25), channel_id=1, replica_groups=mesh['sp'=64,'tp'=16] {'tp'}, dimensions={0} | all-to-all | bytes 1048576 | tf_op jit(solution)/shard_map/all_to_all | solution.py:38
  414.9 1.4 fusion.24
  416.5 16.5 %all_to_all.211 = bf16[16,128,128]{1,2,0:T(8,128)(2,1)S(1)} all-to-all(bf16[16,128,128]{1,2,0:T(8,128)(2,1)S(1)} %broadcast_in_dim.44), channel_id=1, replica_groups=mesh['sp'=64,'tp'=16] {'tp'}, dimensions={0} | all-to-all | bytes 1048576 | tf_op jit(solution)/shard_map/all_to_all | solution.py:38
  435.3 19.6 %all_to_all.212 = bf16[16,128,384]{1,2,0:T(8,128)(2,1)S(1)} all-to-all(bf16[16,128,384]{1,2,0:T(8,128)(2,1)S(1)} %broadcast_in_dim.45), channel_id=1, replica_groups=mesh['sp'=64,'tp'=16] {'tp'}, dimensions={0} | all-to-all | bytes 3145728 | tf_op jit(solution)/shard_map/all_to_all | solution.py:38
  (149 shorter events, 40.8 us)
Async XLA Ops:
  6.5 427.0 %copy-start = (bf16[2048,384]{1,0:T(8,128)(2,1)S(1)}, bf16[2048,384]{1,0:T(8,128)(2,1)}, u32[]{:S(2)}) copy-start(bf16[2048,384]{1,0:T(8,128)(2,1)} %param.25) | copy-start | bytes 4718596
  6.5 21.3 %copy-start.2 = (bf16[256,2048]{1,0:T(8,128)(2,1)S(1)}, bf16[256,2048]{1,0:T(8,128)(2,1)}, u32[]{:S(2)}) copy-start(bf16[256,2048]{1,0:T(8,128)(2,1)} %param.17) | copy-start | bytes 3145732
  6.5 32.3 %copy-start.11 = (bf16[2,2048,16]{1,2,0:T(8,128)(2,1)S(1)}, bf16[2,2048,16]{1,2,0:T(8,128)(2,1)}, u32[]{:S(2)}) copy-start(bf16[2,2048,16]{1,2,0:T(8,128)(2,1)} %param.21) | copy-start | bytes 393220
  6.5 21.3 %copy-start.12 = (bf16[2,2048,16]{1,2,0:T(8,128)(2,1)S(1)}, bf16[2,2048,16]{1,2,0:T(8,128)(2,1)}, u32[]{:S(2)}) copy-start(bf16[2,2048,16]{1,2,0:T(8,128)(2,1)} %param.22) | copy-start | bytes 393220
  11.5 22.5 %all-to-all-start = ((bf16[16,2,128]{2,1,0:T(2,128)(2,1)}), bf16[16,2,128]{2,1,0:T(2,128)(2,1)S(1)}, u32[]{:S(2)}, u32[]{:S(2)}) async-start(bf16[16,2,128]{2,1,0:T(2,128)(2,1)} %reshape.363), calls=%async_computation | async-start | bytes 16384 | tf_op jit(solution)/shard_map/all_to_all | solution.py:48
  34.0 11.1 %all-to-all-start.1 = ((bf16[16,2,128]{2,1,0:T(2,128)(2,1)}), bf16[16,2,128]{2,1,0:T(2,128)(2,1)S(1)}, u32[]{:S(2)}, u32[]{:S(2)}) async-start(bf16[16,2,128]{2,1,0:T(2,128)(2,1)} %reshape.361), calls=%async_computation.1 | async-start | bytes 16384 | tf_op jit(solution)/shard_map/all_to_all | solution.py:48
  38.9 29.0 %copy-start.4 = (bf16[128,128]{1,0:T(8,128)(2,1)S(1)}, bf16[128,128]{1,0:T(8,128)(2,1)}, u32[]{:S(2)}) copy-start(bf16[128,128]{1,0:T(8,128)(2,1)} %param.16) | copy-start | bytes 98308
  45.1 10.8 %all-to-all-start.2 = ((bf16[16,2,128]{2,1,0:T(2,128)(2,1)}), bf16[16,2,128]{2,1,0:T(2,128)(2,1)S(1)}, u32[]{:S(2)}, u32[]{:S(2)}) async-start(bf16[16,2,128]{2,1,0:T(2,128)(2,1)} %reshape.359), calls=%async_computation.2 | async-start | bytes 16384 | tf_op jit(solution)/shard_map/all_to_all | solution.py:48
  49.8 24.1 %copy-start.8 = (f32[3,2048]{1,0:T(4,128)S(1)}, f32[3,2048]{1,0:T(4,128)}, u32[]{:S(2)}) copy-start(f32[3,2048]{1,0:T(4,128)} %param.18) | copy-start | bytes 73732
  55.9 11.1 %all-to-all-start.3 = ((bf16[16,2,128]{2,1,0:T(2,128)(2,1)}), bf16[16,2,128]{2,1,0:T(2,128)(2,1)S(1)}, u32[]{:S(2)}, u32[]{:S(2)}) async-start(bf16[16,2,128]{2,1,0:T(2,128)(2,1)} %reshape.357), calls=%async_computation.3 | async-start | bytes 16384 | tf_op jit(solution)/shard_map/all_to_all | solution.py:48
  60.8 139.7 %all-gather.2.cloned.1.call-start = ((), (), s32[]{:S(2)}) async-start(), calls=%async_computation.18 | async-start | bytes 2129920 | tf_op jit(solution)/shard_map/all_gather | solution.py:23
  68.9 16.8 %all-to-all-start.4 = ((bf16[16,128,128]{1,2,0:T(8,128)(2,1)}), bf16[16,128,128]{1,2,0:T(8,128)(2,1)S(1)}, u32[]{:S(2)}, u32[]{:S(2)}) async-start(bf16[16,128,128]{1,2,0:T(8,128)(2,1)} %broadcast_in_dim.20), calls=%async_computation.4 | async-start | bytes 1048576 | tf_op jit(solution)/shard_map/all_to_all | solution.py:38
  73.8 19.4 %copy-start.9 = (f32[2,16]{1,0:T(2,128)S(1)}, f32[2,16]{1,0:T(2,128)}, u32[]{:S(2)}) copy-start(f32[2,16]{1,0:T(2,128)} %param.24) | copy-start | bytes 388
  88.3 115.1 %all-to-all-start.5 = ((bf16[16,128,128]{2,1,0:T(8,128)(2,1)}), bf16[16,128,128]{2,1,0:T(8,128)(2,1)S(1)}, u32[]{:S(2)}, u32[]{:S(2)}) async-start(bf16[16,128,128]{2,1,0:T(8,128)(2,1)} %broadcast_in_dim.21), calls=%async_computation.5 | async-start | bytes 1048576 | tf_op jit(solution)/shard_map/all_to_all | solution.py:38
  253.6 10.8 %all-to-all-start.8 = ((f32[16,1,128]{2,1,0:T(1,128)}), f32[16,1,128]{2,1,0:T(1,128)S(1)}, u32[]{:S(2)}, u32[]{:S(2)}) async-start(f32[16,1,128]{2,1,0:T(1,128)} %bitcast.30), calls=%async_computation.8 | async-start | bytes 16384 | tf_op jit(solution)/shard_map/all_to_all | solution.py:131
  258.2 33.3 %copy-start.5 = (bf16[128,128]{1,0:T(8,128)(2,1)S(1)}, bf16[128,128]{1,0:T(8,128)(2,1)}, u32[]{:S(2)}) copy-start(bf16[128,128]{1,0:T(8,128)(2,1)} %param.16) | copy-start | bytes 98308
  264.3 13.8 %all-to-all-start.6 = ((bf16[16,128,128]{2,1,0:T(8,128)(2,1)}), bf16[16,128,128]{2,1,0:T(8,128)(2,1)S(1)}, u32[]{:S(2)}, u32[]{:S(2)}) async-start(bf16[16,128,128]{2,1,0:T(8,128)(2,1)} %bitcast.27), calls=%async_computation.6 | async-start | bytes 1048576 | tf_op jit(solution)/shard_map/all_to_all | solution.py:48
  278.3 27.9 %copy-start.3 = (f32[1,2048]{1,0:T(1,128)S(1)}, f32[1,2048]{1,0:T(1,128)}, u32[]{:S(2)}) copy-start(f32[1,2048]{1,0:T(1,128)} %get-tuple-element.237) | copy-start | bytes 24580
  292.8 16.0 %copy-start.6 = (bf16[128,128]{1,0:T(8,128)(2,1)}, bf16[128,128]{1,0:T(8,128)(2,1)S(1)}, u32[]{:S(2)}) copy-start(bf16[128,128]{1,0:T(8,128)(2,1)S(1)} %fusion.22) | copy-start | bytes 98308
  308.8 13.7 %all-to-all-start.11 = ((bf16[16,128,128]{2,1,0:T(8,128)(2,1)}), bf16[16,128,128]{2,1,0:T(8,128)(2,1)S(1)}, u32[]{:S(2)}, u32[]{:S(2)}) async-start(bf16[16,128,128]{2,1,0:T(8,128)(2,1)} %broadcast_in_dim.24), calls=%async_computation.11 | async-start | bytes 1048576 | tf_op jit(solution)/shard_map/all_to_all | solution.py:38
  370.2 11.6 %all-to-all-start.14 = ((f32[16,1,128]{2,1,0:T(1,128)}), f32[16,1,128]{2,1,0:T(1,128)S(1)}, u32[]{:S(2)}, u32[]{:S(2)}) async-start(f32[16,1,128]{2,1,0:T(1,128)} %bitcast.49), calls=%async_computation.14 | async-start | bytes 16384 | tf_op jit(solution)/shard_map/all_to_all | solution.py:131
  375.0 39.9 %copy-start.7 = (bf16[128,128]{1,0:T(8,128)(2,1)S(1)}, bf16[128,128]{1,0:T(8,128)(2,1)}, u32[]{:S(2)}) copy-start(bf16[128,128]{1,0:T(8,128)(2,1)} %copy-done.6) | copy-start | bytes 98308
  381.8 16.7 %all-to-all-start.12 = ((bf16[16,128,128]{2,1,0:T(8,128)(2,1)}), bf16[16,128,128]{2,1,0:T(8,128)(2,1)S(1)}, u32[]{:S(2)}, u32[]{:S(2)}) async-start(bf16[16,128,128]{2,1,0:T(8,128)(2,1)} %bitcast.46), calls=%async_computation.12 | async-start | bytes 1048576 | tf_op jit(solution)/shard_map/all_to_all | solution.py:48
  432.9 1.4 copy-start.10
  435.0 19.9 %copy-start.1 = (bf16[6144,128]{1,0:T(8,128)(2,1)S(1)}, bf16[6144,128]{1,0:T(8,128)(2,1)}, u32[]{:S(2)}) copy-start(bf16[6144,128]{1,0:T(8,128)(2,1)} %param.27) | copy-start | bytes 4718596
Sparse Core Ops, SparseCore 0:
  68.0 132.4 all-gather.1
where the time goes:
time: 466 us; the launch traced here: 463 us
  waiting for transfers between devices  177 us (38%)
  blocking collectives  102 us (22%)
  starting transfers between devices  64.8 us (14%)
  matrix products  43.5 us (9%)
  other arithmetic  33.1 us (7%)
  local copies, waits for them, and re-layouts  28.2 us (6%)
  between operations  13.8 us (3%)
    all_gather x1, waiting for transfers between devices, in_one_piece(): result, at, outs = (lax.all_gather(both, axis, axis=dim, tiled=True), 0, [])  107 us
    all_to_all x5, blocking collectives, from_everyone(): return lax.all_to_all(copies, axis, split_axis=0, concat_axis=0, tiled=True)  78.4 us
    all_to_all x6, starting transfers between devices, regroup(): lax.all_to_all(shortened(items), 'tp', split_axis=0, concat_axis=1, tiled...  40.8 us
    all_to_all x6, waiting for transfers between devices, regroup(): lax.all_to_all(shortened(items), 'tp', split_axis=0, concat_axis=1, tiled...  40.5 us
    all_to_all x2, blocking collectives, finish(): lax.all_to_all(maxima.reshape(QH, row_count), 'tp', split_axis=0, concat_...  23.8 us
    all_to_all x3, waiting for transfers between devices, from_everyone(): return lax.all_to_all(copies, axis, split_axis=0, concat_axis=0, tiled=True)  20.1 us
    dot_general x8, matrix products, attend(): jnp.einsum('grkt,kgd->grdt', expwts.astype(jnp.bfloat16), value_heads, pr...  18.5 us
    reduce_sum x8, other arithmetic, attend(): totals = totals * shrink + jnp.sum(expwts, axis=2)  16.1 us
  transfers between devices with their start and end apart: 12, of which 11 were waited for; matrix products, arithmetic and copies ran while one was open for 3% of the time, Pallas kernels for 0%

commit v1 on v0

v1 whole, which is shorter than its diff:
```python
import math

import jax
import jax.numpy as jnp
from jax import lax
from jax.experimental import pallas as pl
from jax.experimental.pallas import tpu as pltpu
from jax.sharding import PartitionSpec as P

MESH = pl.DeviceIdType.MESH
D = 2048
HEAD = 128
EPSILON = 1e-06
LOG2E = 1.4426950408889634
F32 = jnp.float32
BF16 = jnp.bfloat16
NZ = 32
X0, X1, X2, A0, A1, H0 = range(6)
C0, Q0, Q1, O0, O1, M0, M1 = range(7)
FULL = [(dy, dx) for dy in range(4) for dx in range(4) if dy or dx]
HALF = [(dy, dx) for dy in range(2) for dx in range(4) if dy or dx]


def slot(d):
    return (d + 1) % NZ


def kernel(
    x_hbm, enc_hbm, gain_ref, egain_ref, wq_hbm, wk_hbm, wv_hbm, wo_hbm, sharp_ref, wg_hbm, wu_hbm, wd_hbm,
    out_ref,
    x_v, enc_v, wkv, wq_v, wo_v, wg_v, wu_v, wd_v,
    comp, rbuf, kvbuf, xbuf, qown, qbuf, osend, mlsend, obuf, mlbuf, aown, abuf, sown, hown, hbuf,
    o_acc, m_acc, l_acc, cvec,
    lsem, psend, precv, hsend, hrecv, zsend_sem, zrecv_sem,
):
    t = lax.axis_index("tp")
    s = lax.axis_index("sp")
    y, x = t // 4, t % 4
    g, r = t // 8, t % 8
    z, c = s // 2, s % 2

    locals_ = {}

    def fetch(i, src, dst):
        cp = pltpu.make_async_copy(src, dst, lsem.at[i])
        cp.start()
        locals_[i] = cp

    fetch(0, enc_hbm, enc_v)
    for l in range(2):
        fetch(1 + 2 * l, wk_hbm.at[l], wkv.at[pl.ds(32 * l, 16)])
        fetch(2 + 2 * l, wv_hbm.at[l], wkv.at[pl.ds(32 * l + 16, 16)])
    fetch(5, x_hbm, x_v)
    fetch(6, wq_hbm, wq_v)
    fetch(7, wo_hbm, wo_v)
    fetch(8, wg_hbm, wg_v)
    fetch(9, wu_hbm, wu_v)
    fetch(10, wd_hbm, wd_v)

    def plane_peer(dy, dx):
        return ((y + dy) % 4) * 4 + (x + dx) % 4

    def half_peer(dy, dx):
        return g * 8 + ((y % 2 + dy) % 2) * 4 + (x + dx) % 4

    def z_peer(dz):
        return ((z + dz + NZ) % NZ) * 2 + c

    partner = z * 2 + (1 - c)
    barrier = pltpu.get_barrier_semaphore()
    for dy, dx in FULL:
        pl.semaphore_signal(barrier, inc=1, device_id={"tp": plane_peer(dy, dx)}, device_id_type=MESH)
    for dz in (-4, -2, -1, 1, 2, 4):
        pl.semaphore_signal(barrier, inc=1, device_id={"sp": z_peer(dz)}, device_id_type=MESH)
    pl.semaphore_signal(barrier, inc=1, device_id={"sp": partner}, device_id_type=MESH)

    pending = []

    def plane_send(e, src, dst):
        for dy, dx in FULL:
            d = dy * 4 + dx
            cp = pltpu.make_async_remote_copy(
                src_ref=src, dst_ref=dst, send_sem=psend.at[e, d], recv_sem=precv.at[e, d],
                device_id={"tp": plane_peer(dy, dx)}, device_id_type=MESH,
            )
            cp.start()
            pending.append(cp)

    def plane_wait(e, dst_of):
        for dy, dx in FULL:
            d = dy * 4 + dx
            source = ((y - dy + 4) % 4) * 4 + (x - dx + 4) % 4
            ref = dst_of(source)
            pltpu.make_async_remote_copy(
                src_ref=ref, dst_ref=ref, send_sem=psend.at[e, d], recv_sem=precv.at[e, d],
                device_id={"tp": source}, device_id_type=MESH,
            ).wait_recv()

    def half_send(e, src_of, dst):
        for dy, dx in HALF:
            d = dy * 4 + dx
            peer = half_peer(dy, dx)
            cp = pltpu.make_async_remote_copy(
                src_ref=src_of(peer % 8), dst_ref=dst, send_sem=hsend.at[e, d], recv_sem=hrecv.at[e, d],
                device_id={"tp": peer}, device_id_type=MESH,
            )
            cp.start()
            pending.append(cp)

    def half_wait(e, dst_of):
        for dy, dx in HALF:
            d = dy * 4 + dx
            source = ((y % 2 - dy + 2) % 2) * 4 + (x - dx + 4) % 4
            ref = dst_of(source)
            pltpu.make_async_remote_copy(
                src_ref=ref, dst_ref=ref, send_sem=hsend.at[e, d], recv_sem=hrecv.at[e, d],
                device_id={"tp": g * 8 + source}, device_id_type=MESH,
            ).wait_recv()

    counts = [0, 0]

    def z_copy(l, d, dz, device):
        k = counts[l]
        counts[l] += 1
        cp = pltpu.make_async_remote_copy(
            src_ref=kvbuf.at[l, slot(d), c], dst_ref=kvbuf.at[l, slot(d - dz), c],
            send_sem=zsend_sem.at[l, k], recv_sem=zrecv_sem.at[l, slot(d - dz) * 2 + c],
            device_id={"sp": device}, device_id_type=MESH,
        )
        cp.start()
        pending.append(cp)

    def z_wait(l, d, cc):
        ref = kvbuf.at[l, slot(d), cc]
        pltpu.make_async_remote_copy(
            src_ref=ref, dst_ref=ref, send_sem=zsend_sem.at[l, 0], recv_sem=zrecv_sem.at[l, slot(d) * 2 + cc],
            device_id={"sp": partner}, device_id_type=MESH,
        ).wait_recv()

    def z_near(l, d):
        z_copy(l, d, 1, z_peer(1))
        z_copy(l, d, -1, z_peer(-1))
        if d in (0, -4, -8, -12):
            z_copy(l, d, 2, z_peer(2))
        if d in (0, 4, 8, 12):
            z_copy(l, d, -2, z_peer(-2))
        z_copy(l, d, 0, partner)

    def z_start(l):
        z_copy(l, 0, 4, z_peer(4))
        z_copy(l, 0, -4, z_peer(-4))
        z_near(l, 0)

    def z_jump(l, k):
        z_wait(l, -4 * k, c)
        if k < 4:
            z_copy(l, -4 * k, 4, z_peer(4))
        z_near(l, -4 * k)
        if k < 4:
            z_wait(l, 4 * k, c)
            if k < 3:
                z_copy(l, 4 * k, -4, z_peer(-4))
            z_near(l, 4 * k)

    def z_neighbours(l, d):
        near = [d - 1, d + 1]
        if d in (0, -4, -8, -12):
            near.append(d - 2)
        if d in (0, 4, 8, 12):
            near.append(d + 2)
        for e in near:
            z_wait(l, e, c)
            z_copy(l, e, 0, partner)

    JUMPS = (0, -4, 4, -8, 8, -12, 12, -16)

    locals_[0].wait()
    for i in range(1, 5):
        locals_[i].wait()
    wkv[pl.ds(64, 64), :] = jnp.zeros((64, D), BF16)
    enc = enc_v[...].astype(F32)
    scale = lax.rsqrt(jnp.mean(enc * enc, axis=1, keepdims=True) + EPSILON)
    products = []
    for l in range(2):
        normed = (enc * egain_ref[pl.ds(l, 1), :]).astype(BF16)
        products.append(
            lax.dot_general(normed, wkv[...], (((1,), (1,)), ((), ())), preferred_element_type=F32)
        )
    lane = lax.broadcasted_iota(jnp.int32, (256, 128), 1)
    comp[...] = (jnp.where(lane < 32, products[0], products[1]) * scale).astype(BF16)
    pl.semaphore_wait(barrier, len(FULL) + 7)
    half_send(C0, lambda p: comp.at[pl.ds(pl.multiple_of(p * 32, 32), 32)], rbuf.at[pl.ds(pl.multiple_of(r * 32, 32), 32)])
    rbuf[pl.ds(pl.multiple_of(r * 32, 32), 32), :] = comp[pl.ds(pl.multiple_of(r * 32, 32), 32), :]

    def columns(ref, who, width):
        return ref.at[:, pl.ds(pl.multiple_of(who * width, width), width)]

    locals_[5].wait()
    plane_send(X0, x_v, columns(xbuf.at[0], t, 128))
    columns(xbuf.at[0], t, 128)[...] = x_v[...]

    half_wait(C0, lambda p: rbuf.at[pl.ds(pl.multiple_of(p * 32, 32), 32)])
    row = lax.broadcasted_iota(jnp.int32, (128, 512), 0)
    col = lax.broadcasted_iota(jnp.int32, (128, 512), 1)
    spread = jnp.where((row // 16 == col // 128) & (row % 16 == col % 16), 1.0, 0.0).astype(BF16)
    wide = jnp.dot(rbuf[...], spread, preferred_element_type=F32)
    row = lax.broadcasted_iota(jnp.int32, (256, 512), 0)
    col = lax.broadcasted_iota(jnp.int32, (256, 512), 1)
    wide = jnp.where(row // 32 == (col % 128) // 16, wide, 0.0)
    chunk = jnp.sum(wide.reshape(8, 32, 512), axis=0).astype(BF16)
    kvbuf[0, slot(0), c] = chunk[:, :256]
    kvbuf[1, slot(0), c] = chunk[:, 256:]
    z_start(0)

    def project(l, e):
        plane_wait(e, lambda p: columns(xbuf.at[l], p, 128))
        stream = xbuf[l].astype(F32)
        factor = lax.rsqrt(jnp.mean(stream * stream, axis=1, keepdims=True) + EPSILON)
        normed = (stream * gain_ref[pl.ds(l, 1), :]).astype(BF16)
        return normed, factor

    def queries(l):
        normed, factor = project(l, (X0, X1)[l])
        qown[l] = (jnp.dot(normed, wq_v[l], preferred_element_type=F32) * factor).astype(BF16)
        half_send((Q0, Q1)[l], lambda p: qown.at[l], qbuf.at[l, r])
        qbuf[l, r] = qown[l]

    def attention(l):
        for h in range(8):
            value = sharp_ref[l, g * 8 + h] * (HEAD**-0.5 * LOG2E)
            cvec[:, pl.ds(h * 128, 128)] = jnp.full((1, 128), value, F32)
        m_acc[...] = jnp.full((1, 1024), -1e30, F32)
        l_acc[...] = jnp.zeros((1, 1024), F32)
        o_acc[...] = jnp.zeros((128, 1024), F32)

        def block(j, carry):
            kv = kvbuf[l, pl.ds(4 * j, 4)].reshape(256, 256)
            q = qbuf[l].reshape(1024, 128)
            scores = lax.dot_general(kv[:, :128], q, (((1,), (1,)), ((), ())), preferred_element_type=F32)
            scores = scores * cvec[...]
            m_old = m_acc[...]
            m_new = jnp.maximum(m_old, jnp.max(scores, axis=0, keepdims=True))
            p = jnp.exp2(scores - m_new)
            shrink = jnp.exp2(m_old - m_new)
            m_acc[...] = m_new
            l_acc[...] = l_acc[...] * shrink + jnp.sum(p, axis=0, keepdims=True)
            o_acc[...] = o_acc[...] * shrink + lax.dot_general(
                kv[:, 128:], p.astype(BF16), (((0,), (0,)), ((), ())), preferred_element_type=F32
            )
            return carry

        lax.fori_loop(0, 8, block, 0)
        for h in range(8):
            at = pl.ds(h * 128, 128)
            osend[l, h] = (o_acc[:, at] / l_acc[:, at]).astype(BF16)
            mlsend[l, h, pl.ds(0, 1), :] = m_acc[:, at]
            mlsend[l, h, pl.ds(1, 7), :] = jnp.broadcast_to(l_acc[:, at], (7, 128))
        half_send((O0, O1)[l], lambda p: osend.at[l, p], obuf.at[l, r])
        half_send((M0, M1)[l], lambda p: mlsend.at[l, p], mlbuf.at[l, r])
        obuf[l, r] = osend[l, r]
        mlbuf[l, r] = mlsend[l, r]

    def merge(l):
        half_wait((O0, O1)[l], lambda p: obuf.at[l, p])
        half_wait((M0, M1)[l], lambda p: mlbuf.at[l, p])
        ml = mlbuf[l]
        maxima, totals = ml[:, 0:1, :], ml[:, 1:2, :]
        mixing = jnp.exp2(maxima - jnp.max(maxima, axis=0, keepdims=True)) * totals
        mixing = mixing / jnp.sum(mixing, axis=0, keepdims=True)
        merged = jnp.sum(obuf[l].astype(F32) * mixing, axis=0)
        aown[l] = merged.T.astype(BF16)
        plane_send((A0, A1)[l], aown.at[l], columns(abuf.at[l], t, 128))
        columns(abuf.at[l], t, 128)[...] = aown[l]

    def output(l, previous):
        plane_wait((A0, A1)[l], lambda p: columns(abuf.at[l], p, 128))
        branch = jnp.dot(abuf[l], wo_v[l], preferred_element_type=F32)
        sown[l] = (previous.astype(F32) + branch).astype(BF16)
        plane_send((X1, X2)[l], sown.at[l], columns(xbuf.at[l + 1], t, 128))
        columns(xbuf.at[l + 1], t, 128)[...] = sown[l]

    z_jump(0, 1)
    locals_[6].wait()
    queries(0)
    for k in (2, 3, 4):
        z_jump(0, k)
    for d in JUMPS:
        z_neighbours(0, d)
    z_start(1)
    for d in range(NZ):
        z_wait(0, d, 1 - c)
    half_wait(Q0, lambda p: qbuf.at[0, p])
    attention(0)
    z_jump(1, 1)
    z_jump(1, 2)
    merge(0)
    z_jump(1, 3)
    z_jump(1, 4)
    locals_[7].wait()
    output(0, x_v[...])
    for d in JUMPS:
        z_neighbours(1, d)
    queries(1)
    for d in range(NZ):
        z_wait(1, d, 1 - c)
    half_wait(Q1, lambda p: qbuf.at[1, p])
    attention(1)
    merge(1)
    output(1, sown[0])

    normed, factor = project(2, X2)
    locals_[8].wait()
    locals_[9].wait()
    gate = jnp.dot(normed, wg_v[...], preferred_element_type=F32) * factor
    up = jnp.dot(normed, wu_v[...], preferred_element_type=F32) * factor
    hown[...] = (gate / (1.0 + jnp.exp(-gate)) * up).astype(BF16)
    plane_send(H0, hown, columns(hbuf, t, 384))
    columns(hbuf, t, 384)[...] = hown[...]
    plane_wait(H0, lambda p: columns(hbuf, p, 384))
    locals_[10].wait()
    branch = jnp.dot(hbuf[...], wd_v[...], preferred_element_type=F32)
    out_ref[...] = (sown[1].astype(F32) + branch).astype(BF16)
    for cp in pending:
        cp.wait_send()


def per_device(x, enc, gains, egains, wq, wk, wv, wo, sharp, wg, wu, wd):
    anywhere = pl.BlockSpec(memory_space=pl.ANY)
    vmem = pl.BlockSpec(memory_space=pltpu.VMEM)
    smem = pl.BlockSpec(memory_space=pltpu.SMEM)
    scratch = [
        pltpu.VMEM((128, 128), BF16),
        pltpu.VMEM((256, D), BF16),
        pltpu.VMEM((128, D), BF16),
        pltpu.VMEM((2, D, 128), BF16),
        pltpu.VMEM((2, D, 128), BF16),
        pltpu.VMEM((D, 384), BF16),
        pltpu.VMEM((D, 384), BF16),
        pltpu.VMEM((6144, 128), BF16),
        pltpu.VMEM((256, 128), BF16),
        pltpu.VMEM((256, 128), BF16),
        pltpu.VMEM((2, NZ, 2, 32, 256), BF16),
        pltpu.VMEM((3, 128, D), BF16),
        pltpu.VMEM((2, 128, 128), BF16),
        pltpu.VMEM((2, 8, 128, 128), BF16),
        pltpu.VMEM((2, 8, 128, 128), BF16),
        pltpu.VMEM((2, 8, 8, 128), F32),
        pltpu.VMEM((2, 8, 128, 128), BF16),
        pltpu.VMEM((2, 8, 8, 128), F32),
        pltpu.VMEM((2, 128, 128), BF16),
        pltpu.VMEM((2, 128, D), BF16),
        pltpu.VMEM((2, 128, 128), BF16),
        pltpu.VMEM((128, 384), BF16),
        pltpu.VMEM((128, 6144), BF16),
        pltpu.VMEM((128, 1024), F32),
        pltpu.VMEM((1, 1024), F32),
        pltpu.VMEM((1, 1024), F32),
        pltpu.VMEM((1, 1024), F32),
        pltpu.SemaphoreType.DMA((11,)),
        pltpu.SemaphoreType.DMA((6, 16)),
        pltpu.SemaphoreType.DMA((6, 16)),
        pltpu.SemaphoreType.DMA((7, 8)),
        pltpu.SemaphoreType.DMA((7, 8)),
        pltpu.SemaphoreType.DMA((2, 64)),
        pltpu.SemaphoreType.DMA((2, 64)),
    ]
    return pl.pallas_call(
        kernel,
        out_shape=jax.ShapeDtypeStruct((128, 128), BF16),
        in_specs=[anywhere, anywhere, vmem, vmem, anywhere, anywhere, anywhere, anywhere, smem] + [anywhere] * 3,
        out_specs=vmem,
        scratch_shapes=scratch,
        compiler_params=pltpu.CompilerParams(
            collective_id=0, has_side_effects=True, vmem_limit_bytes=60 * 1024 * 1024
        ),
        name="decoder",
    )(x, enc, gains, egains, wq, jnp.swapaxes(wk, 1, 2), jnp.swapaxes(wv, 1, 2), wo, sharp, wg, wu, wd)


def solution(mesh):
    placed = (
        P("sp", "tp"),
        P("sp", None),
        P(),
        P(),
        P(None, None, "tp"),
        P(None, None, "tp"),
        P(None, None, "tp"),
        P(None, None, "tp"),
        P(),
        P(None, "tp"),
        P(None, "tp"),
        P(None, "tp"),
    )
    return jax.shard_map(per_device, mesh=mesh, in_specs=placed, out_specs=P("sp", "tp"), check_vma=False)
```

time: 466 us -> 143 us (0.31)
  the two profiles are of different devices: /device:TPU:2 before, /device:TPU:16 now
where the time goes in v1:
time: 143 us; the launch traced here: 142 us
  Pallas kernels  141 us (99%)
    pallas_call x1, Pallas kernels, per_device(): pl.pallas_call(kernel, out_shape=jax.ShapeDtypeStruct((128, 128), BF16),...  141 us

profile of v1, /device:TPU:16, one launch (start us, length us, event | category | flops | bytes accessed | tf_op | source)
XLA Modules:
  0.0 142.4 jit_solution(2174693028581838443)
XLA Ops:
  0.0 141.1 %decoder.1 = bf16[128,128]{1,0:T(8,128)(2,1)} custom-call(bf16[128,128]{1,0:T(8,128)(2,1)} %x_hbm.1, bf16[256,2048]{1,0:T(8,128)(2,1)} %enc_hbm.1, f32[3,2048]{1,0:T(4,128)} %gain_ref.1, f32[2,2048]{1,0:T(2,128)} %egain_ref.1, bf16[2,2048,128]{2,1,0:T(8,128)(2,1)} %wq_hbm.1, bf16[2,16,2048]{2,1,0:T(8,128)(2,1)} %bitcast.2, bf16[2,16,2048]{2,1,0:T(8,128)(2,1)} %bitcast.3, ...), custom_call_target="tpu_custom_call" | custom-call | tf_op jit(solution)/shard_map/decoder/pallas_call | solution.py:367
  141.1 1.4 copy.14
